TPU v7x, 32 devices: a whole 2x2x4 slice. The times are simulated.
32 devices in a mesh: grp: 2 (over y), sp: 4 (over z), tp: 4 (over x, core).
Axes of the slice: x: 2, y: 2, z: 4, core: 2. Of those that a mesh axis runs over, the one named last changes fastest.
Arguments:
- resid: bfloat16 [5120, 2048], P(('grp', 'sp'), 'tp'), parts along dimension 0, may hold values from -6 to 6
- queries: bfloat16 [5120, 2048], P(('grp', 'sp'), 'tp'), parts along dimension 0, may hold values from -150 to 150
- keys_values: bfloat16 [5120, 8, 128], P(('grp', 'sp'), 'tp'), parts along dimension 0, may hold values from -4.5 to 4.5
- sink: float32 [32], P('tp'), may hold values from 3 to 7
- out_weight: bfloat16 [2048, 2048], P('tp'), may hold values from -2.390625 to 2.390625
- norm_gain: float32 [2048], replicated, may hold values from 0.1 to 1.9
- gate_weight: bfloat16 [2048, 5632], P('sp', 'tp'), may hold values from -0.125 to 0.125
- up_weight: bfloat16 [2048, 5632], P('sp', 'tp'), may hold values from -0.125 to 0.125
- down_weight: bfloat16 [5632, 2048], P('tp', 'sp'), may hold values from -0.078125 to 0.078125
Outputs:
- mixed: bfloat16 [5120, 2048], P(('grp', 'sp'), 'tp'), parts along dimension 0
There are 2 independent parts, one for each index of `grp`. A program takes and returns all parts, laid end to end along the dimension named above; an argument that names none is the same for every part. Nothing has to cross between parts.
All inputs are finite; a program needn't handle non-finite values.
Results may differ from a plain program's by a relative error of at most 0.008.
Values may be sent and summed in bfloat16 or wider, within the bound.
A program may use at most 128 MiB of HBM per device.

v0:
```python
import jax
import jax.numpy as jnp
from jax import lax
from jax.sharding import PartitionSpec as P

HEAD_DIM = 64
WINDOW = 128
GRID_W = 64


def with_halo(cells, sides, width):
    for axis, dim in sides:
        count = lax.axis_size(axis)
        ends = count - 1
        head = lax.slice_in_dim(cells, 0, width, axis=dim)
        tail = lax.slice_in_dim(cells, cells.shape[dim] - width, cells.shape[dim], axis=dim)
        cells = jnp.concatenate(
            [
                lax.ppermute(tail, axis, [(i, (i + 1) % count) for i in range(ends)]),
                cells,
                lax.ppermute(head, axis, [((i + 1) % count, i) for i in range(ends)]),
            ],
            axis=dim,
        )
    return cells


def rotate(values, positions):
    quarter = 16
    inverse = 10000.0 ** (-jnp.arange(quarter, dtype=jnp.float32) / quarter)

    def turn(part, place):
        angle = place.astype(jnp.float32)[:, None] * inverse[None, :]
        cosine = jnp.cos(angle)[:, None, :]
        sine = jnp.sin(angle)[:, None, :]
        first, second = (part[..., :quarter], part[..., quarter:])
        return jnp.concatenate(
            [first * cosine - second * sine, second * cosine + first * sine], axis=-1
        )

    grid_row = positions // GRID_W
    grid_col = positions % GRID_W
    return jnp.concatenate(
        [turn(values[..., :32], grid_row), turn(values[..., 32:], grid_col)], axis=-1
    )


def body(
    resid, queries, keys_values, sink, out_weight, norm_gain, gate_weight, up_weight, down_weight
):
    tok = queries.shape[0]
    heads_here = queries.shape[1] // HEAD_DIM
    kv_here = keys_values.shape[1]
    group = heads_here // kv_here
    cols = resid.shape[1]
    offset = lax.axis_index("sp") * tok
    total_tokens = tok * lax.axis_size("sp")
    positions = offset + jnp.arange(tok, dtype=jnp.int32)
    rotated_q = rotate(
        queries.astype(jnp.float32).reshape(tok, heads_here, HEAD_DIM), positions
    ).astype(jnp.bfloat16)
    rotated_k = rotate(keys_values[..., :HEAD_DIM].astype(jnp.float32), positions).astype(
        jnp.bfloat16
    )
    joined = jnp.concatenate([rotated_k, keys_values[..., HEAD_DIM:]], axis=-1)
    padded = with_halo(joined, (("sp", 0),), WINDOW)
    blocks = tok // WINDOW
    key_blocks = jnp.stack(
        [padded[index * WINDOW : index * WINDOW + 3 * WINDOW] for index in range(blocks)]
    )
    grouped = rotated_q.reshape(blocks, WINDOW, kv_here, group, HEAD_DIM)
    scores = jnp.einsum(
        "nqkgd,njkd->nkgqj", grouped, key_blocks[..., :HEAD_DIM], preferred_element_type=jnp.float32
    ) * HEAD_DIM ** (-0.5)
    block_start = offset + WINDOW * jnp.arange(blocks, dtype=jnp.int32)
    query_pos = block_start[:, None] + jnp.arange(WINDOW, dtype=jnp.int32)[None, :]
    key_pos = block_start[:, None] - WINDOW + jnp.arange(3 * WINDOW, dtype=jnp.int32)[None, :]
    valid = (
        (jnp.abs(query_pos[:, :, None] - key_pos[:, None, :]) <= WINDOW)
        & (key_pos[:, None, :] >= 0)
        & (key_pos[:, None, :] < total_tokens)
    )
    scores = jnp.where(valid[:, None, None], scores, jnp.float32(-1e30))
    sink_grid = sink.reshape(kv_here, group)[None, :, :, None]
    top = jnp.maximum(jnp.max(scores, axis=-1), sink_grid)
    expo = jnp.exp(scores - top[..., None])
    denom = jnp.sum(expo, axis=-1) + jnp.exp(sink_grid - top)
    probs = (expo / denom[..., None]).astype(jnp.bfloat16)
    attended = jnp.einsum(
        "nkgqj,njkd->nqkgd", probs, key_blocks[..., HEAD_DIM:], preferred_element_type=jnp.float32
    )
    attended = attended.astype(jnp.bfloat16).reshape(tok, heads_here * HEAD_DIM)
    attn_rows, resid_rows = (
        lax.all_to_all(attended, "tp", split_axis=0, concat_axis=1, tiled=True),
        lax.all_to_all(resid, "tp", split_axis=0, concat_axis=1, tiled=True),
    )
    whole_out = lax.all_gather(out_weight, "tp", axis=0, tiled=True)
    stream_part = (
        resid_rows.astype(jnp.float32)
        + jnp.dot(attn_rows, whole_out, preferred_element_type=jnp.float32)
    ).astype(jnp.bfloat16)
    stream = lax.all_gather(stream_part, "tp", axis=0, tiled=True)
    stream_cols = lax.dynamic_slice_in_dim(stream, lax.axis_index("tp") * cols, cols, 1)
    widened = stream.astype(jnp.float32)
    normed = (
        widened * lax.rsqrt(jnp.mean(widened * widened, axis=-1, keepdims=True) + 1e-06) * norm_gain
    ).astype(jnp.bfloat16)
    gate = jnp.dot(
        normed,
        lax.all_gather(gate_weight, "sp", axis=0, tiled=True),
        preferred_element_type=jnp.float32,
    )
    up = jnp.dot(
        normed,
        lax.all_gather(up_weight, "sp", axis=0, tiled=True),
        preferred_element_type=jnp.float32,
    )
    hidden = (jax.nn.silu(gate) * up).astype(jnp.bfloat16)
    terms = jnp.dot(
        hidden,
        lax.all_gather(down_weight, "sp", axis=1, tiled=True),
        preferred_element_type=jnp.float32,
    )
    summed = lax.psum_scatter(
        terms.astype(jnp.bfloat16), "tp", scatter_dimension=1, tiled=True
    ).astype(jnp.float32)
    return (stream_cols.astype(jnp.float32) + summed).astype(jnp.bfloat16)


def solution(mesh):
    return jax.shard_map(
        body,
        mesh=mesh,
        in_specs=(
            P(("grp", "sp"), "tp"),
            P(("grp", "sp"), "tp"),
            P(("grp", "sp"), "tp", None),
            P("tp"),
            P("tp", None),
            P(),
            P("sp", "tp"),
            P("sp", "tp"),
            P("tp", "sp"),
        ),
        out_specs=P(("grp", "sp"), "tp"),
        check_vma=False,
    )
```

profile of v0, /device:TPU:0, one launch (start us, length us, event | category | flops | bytes accessed | tf_op | source)
XLA Modules:
  0.0 493.6 jit_solution(14125125992527969314)
XLA Ops:
  7.3 1.7 fusion.49
  9.9 5.0 %collective-permute-start = (bf16[128,2,128]{0,2,1:T(8,128)(2,1)S(1)}, bf16[128,2,128]{0,2,1:T(8,128)(2,1)S(1)}, u32[]{:S(2)}, u32[]{:S(2)}) collective-permute-start(bf16[128,2,128]{0,2,1:T(8,128)(2,1)S(1)} %get-tuple-element.12), channel_id=1, source_target_pairs={{0,4},{4,8},{8,12},{1,5},{5,9},{9,13},{2,6},{6,10},{10,14},{3,7},{... | collective-permute-start | bytes 196616 | tf_op jit(solution)/shard_map/ppermute | solution.py:19
  14.9 1.3 collective-permute-start.1
  16.2 3.5 all-to-all-start
  20.6 1.2 fusion.11
  23.0 1.3 fusion.1
  24.4 1.9 fusion
  26.4 2.3 fusion.9
  28.7 1.6 copy.38
  30.3 1.6 all_to_all.26
  31.9 5.0 %all-to-all-done = bf16[4,160,512]{2,1,0:T(8,128)(2,1)S(1)} async-done(((bf16[4,160,512]{2,1,0:T(8,128)(2,1)}), bf16[4,160,512]{2,1,0:T(8,128)(2,1)S(1)}, u32[]{:S(2)}, u32[]{:S(2)}) %all-to-all-start) | async-done | bytes 655392 | tf_op jit(solution)/shard_map/all_to_all | solution.py:95
  36.9 3.5 all-to-all-start.1
  40.8 17.3 %all-to-all-done.1 = bf16[4,160,512]{2,1,0:T(8,128)(2,1)S(1)} async-done(((bf16[4,160,512]{2,1,0:T(8,128)(2,1)}), bf16[4,160,512]{2,1,0:T(8,128)(2,1)S(1)}, u32[]{:S(2)}, u32[]{:S(2)}) %all-to-all-start.1) | async-done | bytes 655392 | tf_op jit(solution)/shard_map/all_to_all | solution.py:94
  58.1 25.6 %all-gather.6.cloned.1.call-done = bf16[2048,2048]{1,0:T(8,128)(2,1)} async-done(((bf16[512,2048]{1,0:T(8,128)(2,1)}), bf16[2048,2048]{1,0:T(8,128)(2,1)}) %all-gather.6.cloned.1.call-update) | async-done | bytes 8388624 | tf_op jit(solution)/shard_map/all_gather | solution.py:97
  83.7 5.7 %fusion.7 = bf16[160,2048]{1,0:T(8,128)(2,1)} fusion(f32[160,2048]{1,0:T(8,128)S(1)} %bitcast.70, bf16[160,2048]{1,0:T(8,128)(2,1)S(1)} %bitcast.71, bf16[2048,2048]{1,0:T(8,128)(2,1)} %all-gather.6.cloned.1.call-done), kind=kOutput, calls=%fused_computation.15 | convolution fusion | flops 1342832640 | bytes 11010048 | tf_op jit(solution)/shard_map/dot_general | solution.py:100
  91.6 23.8 %all-gather.8.cloned.1.call-done = bf16[640,2048]{1,0:T(8,128)(2,1)} async-done(((bf16[160,2048]{1,0:T(8,128)(2,1)}), bf16[640,2048]{1,0:T(8,128)(2,1)}) %all-gather.8.cloned.1.call-update) | async-done | bytes 2621456 | tf_op jit(solution)/shard_map/all_gather | solution.py:102
  115.4 2.3 fusion.2
  117.8 106.0 %all-gather.10.cloned.1.call-done = bf16[2048,1408]{1,0:T(8,128)(2,1)} async-done(((bf16[512,1408]{1,0:T(8,128)(2,1)}), bf16[2048,1408]{1,0:T(8,128)(2,1)}) %all-gather.10.cloned.1.call-update) | async-done | bytes 5767184 | tf_op jit(solution)/shard_map/all_gather | solution.py:110
  223.7 9.5 %fusion.14 = f32[640,1408]{1,0:T(8,128)} fusion(bf16[2048,1408]{1,0:T(8,128)(2,1)} %all-gather.10.cloned.1.call-done, bf16[640,2048]{1,0:T(8,128)(2,1)} %all-gather.8.cloned.1.call-done, f32[2048]{0:T(1024)S(1)} %copy-done.2, f32[640]{0:T(1024)S(1)} %add_rsqrt_fusion), kind=kOutput, calls=%fused_computation.23 | convolution fusion | flops 3696230400 | bytes 12003840 | tf_op jit(solution)/shard_map/dot_general | solution.py:108
  233.2 96.9 %all-gather.12.cloned.1.call-done = bf16[2048,1408]{1,0:T(8,128)(2,1)} async-done(((bf16[512,1408]{1,0:T(8,128)(2,1)}), bf16[2048,1408]{1,0:T(8,128)(2,1)}) %all-gather.12.cloned.1.call-update) | async-done | bytes 5767184 | tf_op jit(solution)/shard_map/all_gather | solution.py:115
  330.1 106.4 %all-gather.14.cloned.1.call-done = bf16[1408,2048]{1,0:T(8,128)(2,1)} async-done(((bf16[1408,512]{1,0:T(8,128)(2,1)}), bf16[1408,2048]{1,0:T(8,128)(2,1)}) %all-gather.14.cloned.1.call-update) | async-done | bytes 5767184 | tf_op jit(solution)/shard_map/all_gather | solution.py:121
  436.5 15.3 %convolution_convert_fusion = bf16[640,2048]{1,0:T(8,128)(2,1)} fusion(bf16[1408,2048]{1,0:T(8,128)(2,1)} %all-gather.14.cloned.1.call-done, bf16[2048,1408]{1,0:T(8,128)(2,1)} %all-gather.12.cloned.1.call-done, f32[640,1408]{1,0:T(8,128)} %fusion.14, bf16[640,2048]{1,0:T(8,128)(2,1)S(1)} %copy-done, f32[2048]{0:T(1024)S(1)} %copy-done.2, ...), kind=kOutput, calls=%fused_computation.13 | convolution fusion | flops 7393935360 | bytes 20392448 | tf_op jit(solution)/shard_map/dot_general | solution.py:119
  451.9 32.8 %reduce-scatter.2.cloned.1.call-done = bf16[640,512]{1,0:T(8,128)(2,1)} async-done(((bf16[640,2048]{1,0:T(8,128)(2,1)}), bf16[640,512]{1,0:T(8,128)(2,1)}) %reduce-scatter.2.cloned.1.call-update) | async-done | bytes 655376 | tf_op jit(solution)/shard_map/reduce_scatter | solution.py:124
  484.7 2.1 add_convert_fusion
  (61 shorter events, 6.3 us)
Async XLA Ops:
  6.5 13.2 %copy-start.1 = (bf16[640,512]{1,0:T(8,128)(2,1)S(1)}, bf16[640,512]{1,0:T(8,128)(2,1)}, u32[]{:S(2)}) copy-start(bf16[640,512]{1,0:T(8,128)(2,1)} %param.10) | copy-start | bytes 1966084
  6.5 77.1 %all-gather.6.cloned.1.call-start = ((), (), s32[]{:S(2)}) async-start(), calls=%async_computation.3 | async-start | bytes 10485760 | tf_op jit(solution)/shard_map/all_gather | solution.py:97
  9.9 12.9 %collective-permute-start = (bf16[128,2,128]{0,2,1:T(8,128)(2,1)S(1)}, bf16[128,2,128]{0,2,1:T(8,128)(2,1)S(1)}, u32[]{:S(2)}, u32[]{:S(2)}) collective-permute-start(bf16[128,2,128]{0,2,1:T(8,128)(2,1)S(1)} %get-tuple-element.12), channel_id=1, source_target_pairs={{0,4},{4,8},{8,12},{1,5},{5,9},{9,13},{2,6},{6,10},{10,14},{3,7},{... | collective-permute-start | bytes 196616 | tf_op jit(solution)/shard_map/ppermute | solution.py:19
  14.9 8.1 %collective-permute-start.1 = (bf16[128,2,128]{0,2,1:T(8,128)(2,1)S(1)}, bf16[128,2,128]{0,2,1:T(8,128)(2,1)S(1)}, u32[]{:S(2)}, u32[]{:S(2)}) collective-permute-start(bf16[128,2,128]{0,2,1:T(8,128)(2,1)S(1)} %get-tuple-element.11), channel_id=1, source_target_pairs={{4,0},{8,4},{12,8},{5,1},{9,5},{13,9},{6,2},{10,6},{14,10},{7,3},{... | collective-permute-start | bytes 196616 | tf_op jit(solution)/shard_map/ppermute | solution.py:21
  16.2 20.7 %all-to-all-start = ((bf16[4,160,512]{2,1,0:T(8,128)(2,1)}), bf16[4,160,512]{2,1,0:T(8,128)(2,1)S(1)}, u32[]{:S(2)}, u32[]{:S(2)}) async-start(bf16[4,160,512]{2,1,0:T(8,128)(2,1)} %bitcast), calls=%async_computation | async-start | bytes 1310720 | tf_op jit(solution)/shard_map/all_to_all | solution.py:95
  20.0 2.7 copy-start.3
  36.9 21.1 %all-to-all-start.1 = ((bf16[4,160,512]{2,1,0:T(8,128)(2,1)}), bf16[4,160,512]{2,1,0:T(8,128)(2,1)S(1)}, u32[]{:S(2)}, u32[]{:S(2)}) async-start(bf16[4,160,512]{2,1,0:T(8,128)(2,1)} %all_to_all.26), calls=%async_computation.1 | async-start | bytes 1310720 | tf_op jit(solution)/shard_map/all_to_all | solution.py:94
  40.4 75.0 %all-gather.8.cloned.1.call-start = ((), (), s32[]{:S(2)}) async-start(), calls=%async_computation.4 | async-start | bytes 3276800 | tf_op jit(solution)/shard_map/all_gather | solution.py:102
  89.4 134.3 %copy-start.2 = (f32[2048]{0:T(1024)S(1)}, f32[2048]{0:T(1024)}, u32[]{:S(2)}) copy-start(f32[2048]{0:T(1024)} %param.14) | copy-start | bytes 24580
  89.4 134.3 %all-gather.10.cloned.1.call-start = ((), (), s32[]{:S(2)}) async-start(), calls=%async_computation.5 | async-start | bytes 7208960 | tf_op jit(solution)/shard_map/all_gather | solution.py:110
  90.2 239.9 %all-gather.12.cloned.1.call-start = ((), (), s32[]{:S(2)}) async-start(), calls=%async_computation.6 | async-start | bytes 7208960 | tf_op jit(solution)/shard_map/all_gather | solution.py:115
  90.8 345.8 %all-gather.14.cloned.1.call-start = ((), (), s32[]{:S(2)}) async-start(), calls=%async_computation.7 | async-start | bytes 7208960 | tf_op jit(solution)/shard_map/all_gather | solution.py:121
  91.3 393.3 %reduce-scatter.2.cloned.1.call-start = ((), (), s32[]{:S(2)}) async-start(), calls=%async_computation.8 | async-start | bytes 3276800 | tf_op jit(solution)/shard_map/reduce_scatter | solution.py:124
  117.7 318.8 %copy-start = (bf16[640,2048]{1,0:T(8,128)(2,1)S(1)}, bf16[640,2048]{1,0:T(8,128)(2,1)}, u32[]{:S(2)}) copy-start(bf16[640,2048]{1,0:T(8,128)(2,1)} %all-gather.8.cloned.1.call-done) | copy-start | bytes 7864324
Sparse Core Ops, SparseCore 0:
  8.9 74.7 all-gather.5
  89.6 25.8 all-gather.7
  117.0 106.6 all-gather.9
  225.1 104.9 all-gather.11
  331.5 104.9 all-gather.13
  452.0 32.6 reduce-scatter.1
where the time goes:
time: 494 us
  waiting for transfers between devices  416 us (84%)
  matrix products  34.2 us (7%)
  between operations  13.8 us (3%)
  starting transfers between devices  13.6 us (3%)
  other arithmetic  8.95 us (2%)
  local copies, waits for them, and re-layouts  6.91 us (1%)
    all_gather x1, waiting for transfers between devices, body(): lax.all_gather(down_weight, 'sp', axis=1, tiled=True)  106 us
    all_gather x1, waiting for transfers between devices, body(): lax.all_gather(gate_weight, 'sp', axis=0, tiled=True)  106 us
    all_gather x1, waiting for transfers between devices, body(): lax.all_gather(up_weight, 'sp', axis=0, tiled=True)  96.9 us
    reduce_scatter x1, waiting for transfers between devices, body(): lax.psum_scatter(terms.astype(jnp.bfloat16), 'tp', scatter_dimension=1, t...  32.8 us
    all_gather x1, waiting for transfers between devices, body(): whole_out = lax.all_gather(out_weight, 'tp', axis=0, tiled=True)  25.6 us
    all_gather x1, waiting for transfers between devices, body(): stream = lax.all_gather(stream_part, 'tp', axis=0, tiled=True)  23.8 us
    all_to_all x1, waiting for transfers between devices, body(): lax.all_to_all(attended, 'tp', split_axis=0, concat_axis=1, tiled=True)  17.3 us
    dot_general x1, matrix products, body(): jnp.dot(hidden, lax.all_gather(down_weight, 'sp', axis=1, tiled=True), pr...  15.3 us
  transfers between devices with their start and end apart: 10, of which 8 were waited for; matrix products, arithmetic and copies ran while one was open for 5% of the time, Pallas kernels for 0%

commit v1 on v0

--- a/solution.py
+++ b/solution.py
@@ -94,7 +94,21 @@
         lax.all_to_all(attended, "tp", split_axis=0, concat_axis=1, tiled=True),
         lax.all_to_all(resid, "tp", split_axis=0, concat_axis=1, tiled=True),
     )
-    whole_out = lax.all_gather(out_weight, "tp", axis=0, tiled=True)
+
+    def list_leaves_in(v0, d_out):
+        axis_id = "tp"
+        k_all = jax.lax.axis_size(axis_id)
+        everything = v0
+        arr_out = [(q - 1, q) for q in range(1, k_all)] + [(k_all - 1, 0)]
+        seen = [everything]
+        for _ in range(k_all - 1):
+            everything = jax.lax.ppermute(everything, axis_id, arr_out)
+            seen += [everything]
+        y = jnp.concatenate([*reversed(seen)], axis=d_out)
+        out_arr = jax.lax.axis_index(axis_id)
+        return jnp.roll(y, shift=(out_arr + 1) * everything.shape[d_out], axis=d_out)
+
+    whole_out = list_leaves_in(out_weight, 0)
     stream_part = (
         resid_rows.astype(jnp.float32)
         + jnp.dot(attn_rows, whole_out, preferred_element_type=jnp.float32)

time: 494 us -> 514 us (1.040)
  local copies, waits for them, and re-layouts: 6.91 us -> 22 us
    ppermute x0 -> x3, waiting for transfers between devices: none -> 31.9 us  [list_leaves_in(): everything = jax.lax.ppermute(everything, axis_id, arr_out)]
    all_gather x1 -> x0, waiting for transfers between devices: 25.6 us -> none  [body(): whole_out = lax.all_gather(out_weight, 'tp', axis=0, tiled=True)]
    all_gather x1, waiting for transfers between devices: 96.9 us -> 106 us  [body(): lax.all_gather(up_weight, 'sp', axis=0, tiled=True)]
    all_gather x1, waiting for transfers between devices: 106 us -> 97.1 us  [body(): lax.all_gather(down_weight, 'sp', axis=1, tiled=True)]
    unnamed x14 -> x17, local copies, waits for them, and re-layouts: 0.78 us -> 9.95 us
  transfers between devices with their start and end apart: 10 -> 12, of which waited for: 8 -> 8; matrix products, arithmetic and copies ran while one was open for 5% -> 7% of each run, Pallas kernels for 0% -> 0%
where the time goes in v1:
time: 514 us; the launch traced here: 513 us
  waiting for transfers between devices  419 us (82%)
  matrix products  33.4 us (6%)
  local copies, waits for them, and re-layouts  22 us (4%)
  starting transfers between devices  15 us (3%)
  between operations  13.5 us (3%)
  other arithmetic  10.8 us (2%)
    all_gather x1, waiting for transfers between devices, body(): lax.all_gather(up_weight, 'sp', axis=0, tiled=True)  106 us
    all_gather x1, waiting for transfers between devices, body(): lax.all_gather(gate_weight, 'sp', axis=0, tiled=True)  106 us
    all_gather x1, waiting for transfers between devices, body(): lax.all_gather(down_weight, 'sp', axis=1, tiled=True)  97.1 us
    reduce_scatter x1, waiting for transfers between devices, body(): lax.psum_scatter(terms.astype(jnp.bfloat16), 'tp', scatter_dimension=1, t...  32.8 us
    ppermute x3, waiting for transfers between devices, list_leaves_in(): everything = jax.lax.ppermute(everything, axis_id, arr_out)  31.9 us
    all_gather x1, waiting for transfers between devices, body(): stream = lax.all_gather(stream_part, 'tp', axis=0, tiled=True)  26.9 us
    dot_general x1, matrix products, body(): jnp.dot(hidden, lax.all_gather(down_weight, 'sp', axis=1, tiled=True), pr...  16.1 us
    all_to_all x1, waiting for transfers between devices, body(): lax.all_to_all(attended, 'tp', split_axis=0, concat_axis=1, tiled=True)  15.8 us
  transfers between devices with their start and end apart: 12, of which 8 were waited for; matrix products, arithmetic and copies ran while one was open for 7% of the time, Pallas kernels for 0%

profile of v1, /device:TPU:0, one launch (start us, length us, event | category | flops | bytes accessed | tf_op | source)
XLA Modules:
  0.0 513.4 jit_solution(10297042893464521922)
XLA Ops:
  10.3 4.5 collective-permute-start
  16.1 4.2 all-to-all-start
  20.4 15.9 %collective-permute-done.2 = bf16[512,2048]{1,0:T(8,128)(2,1)S(1)} collective-permute-done((bf16[512,2048]{1,0:T(8,128)(2,1)}, bf16[512,2048]{1,0:T(8,128)(2,1)S(1)}, u32[]{:S(2)}, u32[]{:S(2)}) %collective-permute-start.2) | collective-permute-done | bytes 2097184 | tf_op jit(solution)/shard_map/ppermute | solution.py:105
  44.1 2.3 fusion.3
  46.5 16.0 %collective-permute-done.3 = bf16[512,2048]{1,0:T(8,128)(2,1)} collective-permute-done((bf16[512,2048]{1,0:T(8,128)(2,1)S(1)}, bf16[512,2048]{1,0:T(8,128)(2,1)}, u32[]{:S(2)}, u32[]{:S(2)}) %collective-permute-start.3) | collective-permute-done | bytes 2097184 | tf_op jit(solution)/shard_map/ppermute | solution.py:105
  62.5 1.9 fusion.2
  64.5 3.1 fusion.16
  67.5 2.8 copy.38
  71.9 4.2 all-to-all-start.1
  77.7 15.8 %all-to-all-done.1 = bf16[4,160,512]{2,1,0:T(8,128)(2,1)} async-done(((bf16[4,160,512]{2,1,0:T(8,128)(2,1)}), bf16[4,160,512]{2,1,0:T(8,128)(2,1)}, u32[]{:S(2)}, u32[]{:S(2)}) %all-to-all-start.1) | async-done | bytes 655392 | tf_op jit(solution)/shard_map/all_to_all | solution.py:94
  94.7 1.8 constant_dynamic-update-slice_fusion.8
  96.5 2.0 constant_dynamic-update-slice_fusion.7
  98.9 1.8 constant_dynamic-update-slice_fusion.4
  100.7 1.8 constant_dynamic-update-slice_fusion.3
  103.0 2.5 fusion.12
  107.6 26.9 %all-gather.5.cloned.1.call-done = bf16[640,2048]{1,0:T(8,128)(2,1)} async-done(((bf16[160,2048]{1,0:T(8,128)(2,1)}), bf16[640,2048]{1,0:T(8,128)(2,1)}) %all-gather.5.cloned.1.call-update) | async-done | bytes 2621456 | tf_op jit(solution)/shard_map/all_gather | solution.py:116
  134.5 2.3 fusion.4
  136.8 106.0 %all-gather.7.cloned.1.call-done = bf16[2048,1408]{1,0:T(8,128)(2,1)} async-done(((bf16[512,1408]{1,0:T(8,128)(2,1)}), bf16[2048,1408]{1,0:T(8,128)(2,1)}) %all-gather.7.cloned.1.call-update) | async-done | bytes 5767184 | tf_op jit(solution)/shard_map/all_gather | solution.py:124
  242.7 9.5 %fusion.21 = f32[640,1408]{1,0:T(8,128)} fusion(bf16[2048,1408]{1,0:T(8,128)(2,1)} %all-gather.7.cloned.1.call-done, bf16[640,2048]{1,0:T(8,128)(2,1)} %all-gather.5.cloned.1.call-done, f32[2048]{0:T(1024)S(1)} %copy-done.1, f32[640]{0:T(1024)S(1)} %add_rsqrt_fusion), kind=kOutput, calls=%fused_computation.25 | convolution fusion | flops 3696230400 | bytes 12003840 | tf_op jit(solution)/shard_map/dot_general | solution.py:122
  252.2 97.1 %all-gather.11.cloned.1.call-done = bf16[1408,2048]{1,0:T(8,128)(2,1)} async-done(((bf16[1408,512]{1,0:T(8,128)(2,1)}), bf16[1408,2048]{1,0:T(8,128)(2,1)}) %all-gather.11.cloned.1.call-update) | async-done | bytes 5767184 | tf_op jit(solution)/shard_map/all_gather | solution.py:135
  349.3 106.4 %all-gather.9.cloned.1.call-done = bf16[2048,1408]{1,0:T(8,128)(2,1)} async-done(((bf16[512,1408]{1,0:T(8,128)(2,1)}), bf16[2048,1408]{1,0:T(8,128)(2,1)}) %all-gather.9.cloned.1.call-update) | async-done | bytes 5767184 | tf_op jit(solution)/shard_map/all_gather | solution.py:129
  455.7 16.1 %convolution_convert_fusion = bf16[640,2048]{1,0:T(8,128)(2,1)} fusion(bf16[1408,2048]{1,0:T(8,128)(2,1)} %all-gather.11.cloned.1.call-done, bf16[2048,1408]{1,0:T(8,128)(2,1)} %all-gather.9.cloned.1.call-done, f32[640,1408]{1,0:T(8,128)} %fusion.21, bf16[640,2048]{1,0:T(8,128)(2,1)} %all-gather.5.cloned.1.call-done, f32[2048]{0:T(1024)S(1)} %copy-done.1, ...), kind=kOutput, calls=%fused_computation.15 | convolution fusion | flops 7393935360 | bytes 20392448 | tf_op jit(solution)/shard_map/dot_general | solution.py:133
  471.8 32.8 %reduce-scatter.2.cloned.1.call-done = bf16[640,512]{1,0:T(8,128)(2,1)} async-done(((bf16[640,2048]{1,0:T(8,128)(2,1)}), bf16[640,512]{1,0:T(8,128)(2,1)}) %reduce-scatter.2.cloned.1.call-update) | async-done | bytes 655376 | tf_op jit(solution)/shard_map/reduce_scatter | solution.py:138
  504.6 2.3 add_convert_fusion
  (68 shorter events, 20.2 us)
Async XLA Ops:
  6.5 29.8 %collective-permute-start.2 = (bf16[512,2048]{1,0:T(8,128)(2,1)}, bf16[512,2048]{1,0:T(8,128)(2,1)S(1)}, u32[]{:S(2)}, u32[]{:S(2)}) collective-permute-start(bf16[512,2048]{1,0:T(8,128)(2,1)} %param.13), channel_id=1, source_target_pairs={{0,1},{1,2},{2,3},{3,0},{4,5},{5,6},{6,7},{7,4},{8,9},{9,10},{10,1... | collective-permute-start | bytes 6291464 | tf_op jit(solution)/shard_map/ppermute | solution.py:105
  10.3 33.6 %collective-permute-start = (bf16[128,2,128]{0,2,1:T(8,128)(2,1)}, bf16[128,2,128]{0,2,1:T(8,128)(2,1)S(1)}, u32[]{:S(2)}, u32[]{:S(2)}) collective-permute-start(bf16[128,2,128]{0,2,1:T(8,128)(2,1)} %get-tuple-element.12), channel_id=1, source_target_pairs={{0,4},{4,8},{8,12},{1,5},{5,9},{9,13},{2,6},{6,10},{10,14},{3,7},{... | collective-permute-start | bytes 196616 | tf_op jit(solution)/shard_map/ppermute | solution.py:19
  14.8 29.3 %collective-permute-start.1 = (bf16[128,2,128]{0,2,1:T(8,128)(2,1)}, bf16[128,2,128]{0,2,1:T(8,128)(2,1)S(1)}, u32[]{:S(2)}, u32[]{:S(2)}) collective-permute-start(bf16[128,2,128]{0,2,1:T(8,128)(2,1)} %get-tuple-element.11), channel_id=1, source_target_pairs={{4,0},{8,4},{12,8},{5,1},{9,5},{13,9},{6,2},{10,6},{14,10},{7,3},{... | collective-permute-start | bytes 196616 | tf_op jit(solution)/shard_map/ppermute | solution.py:21
  16.1 55.8 %all-to-all-start = ((bf16[4,160,512]{2,1,0:T(8,128)(2,1)}), bf16[4,160,512]{2,1,0:T(8,128)(2,1)}, u32[]{:S(2)}, u32[]{:S(2)}) async-start(bf16[4,160,512]{2,1,0:T(8,128)(2,1)} %bitcast.72), calls=%async_computation | async-start | bytes 1310720 | tf_op jit(solution)/shard_map/all_to_all | solution.py:95
  36.4 26.1 %collective-permute-start.3 = (bf16[512,2048]{1,0:T(8,128)(2,1)S(1)}, bf16[512,2048]{1,0:T(8,128)(2,1)}, u32[]{:S(2)}, u32[]{:S(2)}) collective-permute-start(bf16[512,2048]{1,0:T(8,128)(2,1)S(1)} %collective-permute-done.2), channel_id=1, source_target_pairs={{0,1},{1,2},{2,3},{3,0},{4,5},{5,6},{6,7},{7,4},{8,9},{9,10},{10,1... | collective-permute-start | bytes 6291464 | tf_op jit(solution)/shard_map/ppermute | solution.py:105
  62.5 32.2 %collective-permute-start.4 = (bf16[512,2048]{1,0:T(8,128)(2,1)}, bf16[512,2048]{1,0:T(8,128)(2,1)}, u32[]{:S(2)}, u32[]{:S(2)}) collective-permute-start(bf16[512,2048]{1,0:T(8,128)(2,1)} %collective-permute-done.3), channel_id=1, source_target_pairs={{0,1},{1,2},{2,3},{3,0},{4,5},{5,6},{6,7},{7,4},{8,9},{9,10},{10,1... | collective-permute-start | bytes 6291464 | tf_op jit(solution)/shard_map/ppermute | solution.py:105
  71.9 21.6 %all-to-all-start.1 = ((bf16[4,160,512]{2,1,0:T(8,128)(2,1)}), bf16[4,160,512]{2,1,0:T(8,128)(2,1)}, u32[]{:S(2)}, u32[]{:S(2)}) async-start(bf16[4,160,512]{2,1,0:T(8,128)(2,1)} %all_to_all.26), calls=%async_computation.1 | async-start | bytes 1310720 | tf_op jit(solution)/shard_map/all_to_all | solution.py:94
  76.1 58.4 %all-gather.5.cloned.1.call-start = ((), (), s32[]{:S(2)}) async-start(), calls=%async_computation.3 | async-start | bytes 3276800 | tf_op jit(solution)/shard_map/all_gather | solution.py:116
  96.5 2.2 copy-start
  105.5 137.3 %copy-start.1 = (f32[2048]{0:T(1024)S(1)}, f32[2048]{0:T(1024)}, u32[]{:S(2)}) copy-start(f32[2048]{0:T(1024)} %param.14) | copy-start | bytes 24580
  105.5 137.3 %all-gather.7.cloned.1.call-start = ((), (), s32[]{:S(2)}) async-start(), calls=%async_computation.4 | async-start | bytes 7208960 | tf_op jit(solution)/shard_map/all_gather | solution.py:124
  106.2 243.1 %all-gather.11.cloned.1.call-start = ((), (), s32[]{:S(2)}) async-start(), calls=%async_computation.6 | async-start | bytes 7208960 | tf_op jit(solution)/shard_map/all_gather | solution.py:135
  107.0 348.7 %all-gather.9.cloned.1.call-start = ((), (), s32[]{:S(2)}) async-start(), calls=%async_computation.5 | async-start | bytes 7208960 | tf_op jit(solution)/shard_map/all_gather | solution.py:129
  107.5 397.0 %reduce-scatter.2.cloned.1.call-start = ((), (), s32[]{:S(2)}) async-start(), calls=%async_computation.7 | async-start | bytes 3276800 | tf_op jit(solution)/shard_map/reduce_scatter | solution.py:138
Sparse Core Ops, SparseCore 0:
  105.6 28.8 all-gather.4
  136.0 106.6 all-gather.6
  244.3 104.9 all-gather.10
  350.7 104.9 all-gather.8
  471.9 32.6 reduce-scatter.1
